TPU v7x, 256 devices: a 4x2x16 block of a 4x16x16 slice. The times are simulated.
256 devices in a mesh: grp: 2 (over y), ep: 32 (over z, core), tp: 4 (over x).
Axes of the slice: x: 4, y: 2, z: 16, core: 2. Of those that a mesh axis runs over, the one named last changes fastest.
The devices are a block of a 4x16x16 slice.
Arguments:
- query_plain: bfloat16 [16384, 512], P(('grp', 'ep'), 'tp'), parts along dimension 0, may hold values from -400 to 400
- query_rotary: bfloat16 [16384, 256], P(('grp', 'ep'), 'tp'), parts along dimension 0, may hold values from -6 to 6
- latent_input: bfloat16 [16384, 256], P(('grp', 'ep')), parts along dimension 0, may hold values from -6 to 6
- rotary_key: bfloat16 [16384, 32], P(('grp', 'ep')), parts along dimension 0, may hold values from -6 to 6
- key_weight: bfloat16 [256, 512], P(None, 'tp'), may hold values from -0.375 to 0.375
- value_weight: bfloat16 [256, 512], P(None, 'tp'), may hold values from -0.375 to 0.375
- latent_gain: bfloat16 [256], replicated, may hold values from 0.099609375 to 1.8984375
- head_gain: bfloat16 [512], P('tp'), may hold values from 0.099609375 to 1.8984375
- out_weight: bfloat16 [512, 2048], P('tp'), may hold values from -0.25 to 0.25
- expert_input: bfloat16 [32768, 2048], P(('grp', 'ep', 'tp')), parts along dimension 0, may hold values from -6 to 6
- expert_gain: bfloat16 [2048], replicated, may hold values from 0.099609375 to 1.8984375
- routes: int32 [32768, 2], P(('grp', 'ep', 'tp')), parts along dimension 0, may hold values from 0 to 31, all different within a row; in each aligned block of 128 rows (0 to 127, 128 to 255, ...) at most 9 rows name the same one
- route_weight: float32 [32768, 2], P(('grp', 'ep', 'tp')), parts along dimension 0, may hold values from 0.1 to 1
- gate_weight: bfloat16 [32, 2048, 3584], P('ep', None, 'tp'), may hold values from -0.125 to 0.125
- up_weight: bfloat16 [32, 2048, 3584], P('ep', None, 'tp'), may hold values from -0.125 to 0.125
- down_weight: bfloat16 [32, 3584, 2048], P('ep', 'tp'), may hold values from -0.09375 to 0.09375
Outputs:
- attended: bfloat16 [16384, 2048], P(('grp', 'ep', 'tp')), parts along dimension 0
- expert_out: bfloat16 [32768, 2048], P(('grp', 'ep', 'tp')), parts along dimension 0
There are 2 independent parts, one for each index of `grp`. A program takes and returns all parts, laid end to end along the dimension named above; an argument that names none is the same for every part. Nothing has to cross between parts.
Inputs may be any that keep to these rules, and one draw needn't show every extreme that they name: `routes`: each of the 128 rows of one device names 2 different experts; no expert is named by more than 9 rows of one device, a bound that some block reaches of some device.
All inputs are finite; a program needn't handle non-finite values.
Results may differ from a plain program's by a relative error of at most 0.012.
Values may be sent and summed in bfloat16 or wider, within the bound.
No kernel may reach another device: no remote copies, remote signals or barrier semaphores. Data moves between devices by JAX's collectives and lax.ppermute only.
A program may use at most 128 MiB of HBM per device.

v0:
```python
import jax
import jax.numpy as jnp
from jax import lax
from jax.sharding import Mesh
from jax.sharding import PartitionSpec as P

PLAIN_DIM = 64
ROTARY_DIM = 32
VALUE_DIM = 64
TOP = 2
EP = ("ep_0", "ep_1")
GRP_EP = ("grp", "ep_0", "ep_1")
GRP_EP_TP = ("grp", "ep_0", "ep_1", "tp")
EPSILON = 1e-06
THETA = 10000.0
key_span = 2048


def sent_together(arrays, axis, dim, along):
    ends, at = ([], 0)
    for a in arrays[:-1]:
        at += a.shape[along]
        ends.append(at)
    both = jnp.concatenate(arrays, axis=along)
    return tuple(jnp.split(lax.all_gather(both, axis, axis=dim, tiled=True), ends, axis=along))


def in_blocks(array, dim, size):
    lengths = array.shape
    tiles = array.reshape(*lengths[:dim], size, lengths[dim] // size, *lengths[dim + 1 :])
    return jnp.moveaxis(tiles, dim, 0)


def sum_at_owner(array, axis, dim):
    size = lax.axis_size(axis)
    tiles = lax.all_to_all(in_blocks(array, dim, size), axis, 0, 0, tiled=True)
    return jnp.sum(tiles.astype(jnp.float32), axis=0)


def joined_along(tiles, dim):
    tiles = jnp.moveaxis(tiles, 0, dim)
    lengths = tiles.shape
    return tiles.reshape(*lengths[:dim], lengths[dim] * lengths[dim + 1], *lengths[dim + 2 :])


def moved_by_axis(tiles, axes, sequence):
    lengths = [lax.axis_size(a) for a in axes]
    tiles = tiles.reshape(*lengths, *tiles.shape[1:])
    for k in sequence:
        tiles = lax.all_to_all(tiles, axes[k], split_axis=k, concat_axis=k, tiled=True)
    return tiles.reshape(-1, *tiles.shape[len(axes) :])


def two_step_exchange(array, groups, sequence, split_dim, concat_dim):
    size = lax.axis_size(groups[0]) * lax.axis_size(groups[1])
    tiles = in_blocks(array, split_dim, size)
    return joined_along(moved_by_axis(tiles, groups, sequence), concat_dim)


def normalize(entries, gain):
    wide = entries.astype(jnp.float32)
    factor = lax.rsqrt(jnp.mean(wide * wide, axis=-1, keepdims=True) + EPSILON)
    return wide * factor * gain.astype(jnp.float32)


def rotate(entries, positions):
    half = entries.shape[-1] // 2
    freqs = THETA ** (-jnp.arange(half, dtype=jnp.float32) / half)
    angle = positions.astype(jnp.float32)[:, None, None] * freqs[None, None, :]
    cosine = jnp.cos(angle)
    sine = jnp.sin(angle)
    first = entries[..., :half].astype(jnp.float32)
    second = entries[..., half:].astype(jnp.float32)
    turned = jnp.concatenate(
        [first * cosine - second * sine, first * sine + second * cosine], axis=-1
    )
    return turned.astype(jnp.bfloat16)


def rounded(entries):
    return lax.optimization_barrier(entries.astype(jnp.bfloat16)).astype(jnp.float32)


def attend(
    query_plain,
    query_rotary,
    latent_input,
    rotary_key,
    key_weight,
    value_weight,
    latent_gain,
    head_gain,
    out_weight,
):
    tokens = query_plain.shape[0]
    heads = key_weight.shape[1] // PLAIN_DIM
    offset = lax.axis_index(EP) * tokens
    positions = offset + jnp.arange(tokens, dtype=jnp.int32)
    last_position = offset + tokens - 1
    latent = normalize(latent_input, latent_gain).astype(jnp.bfloat16)
    key_rotated = rotate(rotary_key.reshape(tokens, 1, ROTARY_DIM), positions).reshape(
        tokens, ROTARY_DIM
    )
    query_rotated = rotate(query_rotary.reshape(tokens, heads, ROTARY_DIM), positions)
    queries = query_plain.reshape(tokens, heads, PLAIN_DIM)
    factor = (PLAIN_DIM + ROTARY_DIM) ** (-0.5)

    def reshape_given(piece):
        key_rows, value_rows, rotated_rows = piece
        count = key_rows.shape[0]
        return (
            key_rows.reshape(count, heads, PLAIN_DIM),
            value_rows.reshape(count, heads, VALUE_DIM),
            rotated_rows,
        )

    def add_keys(carry, unpacked, start):
        total, highest = carry
        keys, values, rotated_rows = unpacked
        count = keys.shape[0]
        scores = jnp.einsum("qhd,khd->qhk", queries, keys, preferred_element_type=jnp.float32)
        scores = scores + jnp.einsum(
            "qhr,kr->qhk", query_rotated, rotated_rows, preferred_element_type=jnp.float32
        )
        scores = scores * factor
        key_positions = start + jnp.arange(count, dtype=jnp.int32)
        allowed = (key_positions[None, :] <= positions[:, None])[:, None, :]
        masked = jnp.where(allowed, scores, -1e30)
        newest = jnp.maximum(highest, jnp.max(masked, axis=-1))
        weights = jnp.where(allowed, jnp.exp(masked - newest[..., None]), 0.0).astype(jnp.bfloat16)
        total = total * jnp.exp(highest - newest)[..., None] + jnp.einsum(
            "qhk,khd->qhd", weights, values, preferred_element_type=jnp.float32
        )
        return (total, newest)

    def make_fold(unpack):

        def guarded(carry, piece, start):

            def compute(state):
                return add_keys(state, unpack(piece), start)

            def keep(state):
                return state

            return lax.cond(start > last_position, keep, compute, carry)

        def fold(carry, piece, start):
            count = piece[0].shape[0]

            def step(index, inner):
                begin = index * key_span
                sliced = tuple(
                    (lax.dynamic_slice_in_dim(member, begin, key_span, 0) for member in piece)
                )
                return guarded(inner, sliced, begin)

            return lax.fori_loop(0, count // key_span, step, carry)

        return fold

    initial = (
        jnp.zeros((tokens, heads, VALUE_DIM), jnp.float32),
        jnp.full((tokens, heads), -1e30, jnp.float32),
    )
    own_keys = jnp.dot(latent, key_weight, preferred_element_type=jnp.float32).astype(jnp.bfloat16)
    own_values = jnp.dot(latent, value_weight, preferred_element_type=jnp.float32).astype(
        jnp.bfloat16
    )
    folded = make_fold(reshape_given)(
        initial, sent_together((own_keys, own_values, key_rotated), EP, 0, 1), jnp.int32(0)
    )
    context = folded[0]
    head_output = (
        normalize(context, head_gain.reshape(heads, VALUE_DIM))
        .astype(jnp.bfloat16)
        .reshape(tokens, heads * VALUE_DIM)
    )
    summed = sum_at_owner(
        rounded(jnp.dot(head_output, out_weight, preferred_element_type=jnp.float32)).astype(
            jnp.bfloat16
        ),
        "tp",
        0,
    )
    return summed.astype(jnp.bfloat16)


def experts(expert_input, expert_gain, routes, route_weight, gate_weight, up_weight, down_weight):
    tokens = expert_input.shape[0]
    features = expert_input.shape[1]
    count_ep = lax.axis_size(EP)
    capacity = min(tokens, max(2, (9 * tokens + 4 * count_ep - 1) // (4 * count_ep)))
    normed = normalize(expert_input, expert_gain).astype(jnp.bfloat16)
    chosen = routes.reshape(-1)
    onehot = (chosen[:, None] == jnp.arange(count_ep, dtype=jnp.int32)[None, :]).astype(jnp.int32)
    ranks = jnp.sum(jnp.cumsum(onehot, axis=0) * onehot, axis=1) - 1
    destination = chosen * capacity + ranks
    outgoing = (
        jnp.zeros((count_ep * capacity, features), jnp.bfloat16)
        .at[destination]
        .set(jnp.repeat(normed, TOP, axis=0))
    )
    gate_local = gate_weight[0]
    up_local = up_weight[0]
    down_local = down_weight[0]
    arrived = two_step_exchange(outgoing, ("ep_0", "ep_1"), (1, 0), 0, 0)
    piece = lax.all_gather(arrived, "tp", axis=0, tiled=True)
    gate = jnp.dot(piece, gate_local, preferred_element_type=jnp.float32)
    upward = jnp.dot(piece, up_local, preferred_element_type=jnp.float32)
    hidden = (jax.nn.silu(gate) * upward).astype(jnp.bfloat16)
    summed = sum_at_owner(
        rounded(jnp.dot(hidden, down_local, preferred_element_type=jnp.float32)).astype(
            jnp.bfloat16
        ),
        "tp",
        0,
    ).astype(jnp.bfloat16)
    returned = lax.all_to_all(summed, EP, split_axis=0, concat_axis=0, tiled=True)
    picked = returned[destination].astype(jnp.float32).reshape(tokens, TOP, features)
    combined = jnp.sum(picked * route_weight[:, :, None], axis=1)
    return combined.astype(jnp.bfloat16)


def body(
    query_plain,
    query_rotary,
    latent_input,
    rotary_key,
    key_weight,
    value_weight,
    latent_gain,
    head_gain,
    out_weight,
    expert_input,
    expert_gain,
    routes,
    route_weight,
    gate_weight,
    up_weight,
    down_weight,
):
    attended = attend(
        query_plain,
        query_rotary,
        latent_input,
        rotary_key,
        key_weight,
        value_weight,
        latent_gain,
        head_gain,
        out_weight,
    )
    expert_out = experts(
        expert_input, expert_gain, routes, route_weight, gate_weight, up_weight, down_weight
    )
    return (attended, expert_out)


def solution(mesh):
    finer = Mesh(
        mesh.devices.reshape(mesh.shape["grp"], 16, 2, mesh.shape["tp"]),
        ("grp", "ep_0", "ep_1", "tp"),
    )
    in_specs = (
        P(GRP_EP, "tp"),
        P(GRP_EP, "tp"),
        P(GRP_EP, None),
        P(GRP_EP, None),
        P(None, "tp"),
        P(None, "tp"),
        P(),
        P("tp"),
        P("tp", None),
        P(GRP_EP_TP, None),
        P(),
        P(GRP_EP_TP, None),
        P(GRP_EP_TP, None),
        P(EP, None, "tp"),
        P(EP, None, "tp"),
        P(EP, "tp", None),
    )
    out_specs = (P(GRP_EP_TP, None), P(GRP_EP_TP, None))
    return jax.shard_map(body, mesh=finer, in_specs=in_specs, out_specs=out_specs, check_vma=False)
```

profile of v0, /device:TPU:33, one launch (start us, length us, event | category | flops | bytes accessed | tf_op | source)
XLA Modules:
  0.0 412.7 jit_solution(7010274078072165320)
XLA Ops:
  14.5 3.2 scatter_custom_fusion
  17.7 1.6 reshape_reshape.6
  20.0 24.7 %all_to_all.32 = bf16[16,2,9,2048]{3,0,2,1:T(8,128)(2,1)S(1)} all-to-all(bf16[16,2,9,2048]{3,0,2,1:T(8,128)(2,1)S(1)} %copy.34), channel_id=1, replica_groups=mesh['grp'=2,'ep_0'=16,'ep_1'=2,'tp'=4] {'ep_1'}, dimensions={1} | all-to-all | bytes 2359296 | tf_op jit(solution)/shard_map/all_to_all | solution.py:50
  46.0 61.2 %all_to_all.33 = bf16[16,2,9,2048]{3,1,2,0:T(2,128)(2,1)S(1)} all-to-all(bf16[16,2,9,2048]{3,1,2,0:T(2,128)(2,1)S(1)} %copy.35), channel_id=1, replica_groups=mesh['grp'=2,'ep_0'=16,'ep_1'=2,'tp'=4] {'ep_0'}, dimensions={0} | all-to-all | bytes 2359296 | tf_op jit(solution)/shard_map/all_to_all | solution.py:50
  111.2 53.7 %all-gather.5.cloned.1.call-done = bf16[1152,2048]{1,0:T(8,128)(2,1)} async-done(((bf16[288,2048]{1,0:T(8,128)(2,1)}), bf16[1152,2048]{1,0:T(8,128)(2,1)}) %all-gather.5.cloned.1.call-update) | async-done | bytes 4718608 | tf_op jit(solution)/shard_map/all_gather | solution.py:208
  164.9 8.1 %fusion.14 = f32[1152,896]{1,0:T(8,128)S(1)} fusion(bf16[1152,2048]{1,0:T(8,128)(2,1)} %all-gather.5.cloned.1.call-done, bf16[1,2048,896]{2,1,0:T(8,128)(2,1)} %param.33), kind=kOutput, calls=%fused_computation.25 | convolution fusion | flops 4227858432 | bytes 12517376 | tf_op jit(solution)/shard_map/dot_general | solution.py:209
  173.0 5.3 %fusion.16 = bf16[1152,896]{1,0:T(8,128)(2,1)S(1)} fusion(bf16[1152,2048]{1,0:T(8,128)(2,1)S(1)} %copy-done.6, bf16[1,2048,896]{2,1,0:T(8,128)(2,1)S(1)} %copy-done.7, f32[1152,896]{1,0:T(8,128)S(1)} %fusion.14), kind=kOutput, calls=%fused_computation.27 | convolution fusion | flops 4234051584 | bytes 14581760 | tf_op jit(solution)/shard_map/dot_general | solution.py:210
  178.4 6.8 %convolution_convert_fusion = bf16[1152,2048]{1,0:T(8,128)(2,1)} fusion(bf16[1152,896]{1,0:T(8,128)(2,1)S(1)} %fusion.16, bf16[1,896,2048]{2,1,0:T(8,128)(2,1)S(1)} %copy-done.8), kind=kOutput, calls=%fused_computation.21 | convolution fusion | flops 4230217728 | bytes 10452992 | tf_op jit(solution)/shard_map/dot_general | solution.py:213
  185.1 5.1 %all-to-all-start.3 = ((bf16[4,288,2048]{2,1,0:T(8,128)(2,1)}), bf16[4,288,2048]{2,1,0:T(8,128)(2,1)}, u32[]{:S(2)}, u32[]{:S(2)}) async-start(bf16[4,288,2048]{2,1,0:T(8,128)(2,1)} %bitcast.70), calls=%async_computation.3 | async-start | bytes 9437184 | tf_op jit(solution)/shard_map/all_to_all | solution.py:36
  190.7 57.7 %all-gather.3.cloned.1.call-done = bf16[8192,288]{0,1:T(8,128)(2,1)} async-done(((bf16[256,288]{0,1:T(8,128)(2,1)}), bf16[8192,288]{0,1:T(8,128)(2,1)}) %all-gather.3.cloned.1.call-update) | async-done | bytes 4718608 | tf_op jit(solution)/shard_map/all_gather | solution.py:25
  249.5 3.9 fusion.47
  253.4 4.5 %while.16 = (s32[]{:T(128)}, f32[256,2,64]{0,2,1:T(8,128)S(1)}, f32[256,2]{0,1:T(2,128)S(1)}, s32[]{:T(128)}, bf16[8192,128]{0,1:T(8,128)(2,1)}, /*index=5*/bf16...) while((s32[]{:T(128)}, f32[256,2,64]{0,2,1:T(8,128)S(1)}, ...), condition=%wide.region_5.6_spmd.clone, body=%wide.region_1.5_spmd.clone.sunk | while | flops 343476992 | bytes 22022456 | solution.py:158
  253.4 4.3 %conditional.3 = ((f32[256,2,64]{0,2,1:T(8,128)S(1)}, f32[256,2]{0,1:T(2,128)S(1)})) conditional(s32[]{:T(128)} %convert_element_type.210, (s32[]{:T(128)}, s32[]{:T(128)}, bf16[8192,128]{0,1:T(8,128)(2,1)}, bf16[256,2,64]{0,2,1:T(8,128)(2,1)S(1)}, bf16[8192,32]{0,1:T(8,128)(2,1)S(1)}, /*index=5*/bf16[256,2,32]{0,2,1:T(8,128)(2,1)S(1)}, ...), branch_computations={%region_2.3_spmd, %region_4.4_spmd} | conditional | flops 343476992 | bytes 22021194 | solution.py:146
  258.1 1.4 convolution_convert_fusion.1
  259.5 3.7 all-to-all-start
  263.2 3.3 reduce_sum.74
  266.6 1.6 all_to_all.24
  268.2 9.7 %all-to-all-done = bf16[4,64,2048]{2,1,0:T(8,128)(2,1)S(1)} async-done(((bf16[4,64,2048]{2,1,0:T(8,128)(2,1)}), bf16[4,64,2048]{2,1,0:T(8,128)(2,1)S(1)}, u32[]{:S(2)}, u32[]{:S(2)}) %all-to-all-start) | async-done | bytes 1048608 | tf_op jit(solution)/shard_map/all_to_all | solution.py:36
  277.9 18.7 %all-to-all-start.4 = ((bf16[32,9,2048]{2,1,0:T(8,128)(2,1)}), bf16[32,9,2048]{2,1,0:T(8,128)(2,1)}, u32[]{:S(2)}, u32[]{:S(2)}) async-start(bf16[32,9,2048]{2,1,0:T(8,128)(2,1)} %all_to_all.24), calls=%async_computation.4 | async-start | bytes 4194304 | tf_op jit(solution)/shard_map/all_to_all | solution.py:219
  297.7 97.7 %all-to-all-done.4 = bf16[32,9,2048]{2,1,0:T(8,128)(2,1)} async-done(((bf16[32,9,2048]{2,1,0:T(8,128)(2,1)}), bf16[32,9,2048]{2,1,0:T(8,128)(2,1)}, u32[]{:S(2)}, u32[]{:S(2)}) %all-to-all-start.4) | async-done | bytes 1179680 | tf_op jit(solution)/shard_map/all_to_all | solution.py:219
  395.3 1.8 all_to_all.26
  397.2 2.3 gather_fusion
  399.5 2.4 reshape.297
  401.9 3.9 multiply_reduce_fusion
  (93 shorter events, 20.1 us)
Async XLA Ops:
  7.2 250.9 %copy-start = (bf16[128,2048]{1,0:T(8,128)(2,1)S(1)}, bf16[128,2048]{1,0:T(8,128)(2,1)}, u32[]{:S(2)}) copy-start(bf16[128,2048]{1,0:T(8,128)(2,1)} %param.28) | copy-start | bytes 1572868
  7.2 157.7 %all-gather.5.cloned.1.call-start = ((), (), s32[]{:S(2)}) async-start(), calls=%async_computation.6 | async-start | bytes 5898240 | tf_op jit(solution)/shard_map/all_gather | solution.py:208
  107.1 2.4 copy-start.11
  107.1 2.4 copy-start.1
  107.1 2.6 copy-start.4
  107.1 2.7 copy-start.9
  107.2 3.0 copy-start.10
  109.3 139.1 %all-gather.3.cloned.1.call-start = ((), (), s32[]{:S(2)}) async-start(), calls=%async_computation.5 | async-start | bytes 4866048 | tf_op jit(solution)/shard_map/all_gather | solution.py:25
  164.9 8.1 %copy-start.6 = (bf16[1152,2048]{1,0:T(8,128)(2,1)S(1)}, bf16[1152,2048]{1,0:T(8,128)(2,1)}, u32[]{:S(2)}) copy-start(bf16[1152,2048]{1,0:T(8,128)(2,1)} %all-gather.5.cloned.1.call-done) | copy-start | bytes 14155780
  164.9 8.1 %copy-start.7 = (bf16[1,2048,896]{2,1,0:T(8,128)(2,1)S(1)}, bf16[1,2048,896]{2,1,0:T(8,128)(2,1)}, u32[]{:S(2)}) copy-start(bf16[1,2048,896]{2,1,0:T(8,128)(2,1)} %param.34) | copy-start | bytes 11010052
  173.0 5.3 %copy-start.8 = (bf16[1,896,2048]{2,1,0:T(8,128)(2,1)S(1)}, bf16[1,896,2048]{2,1,0:T(8,128)(2,1)}, u32[]{:S(2)}) copy-start(bf16[1,896,2048]{2,1,0:T(8,128)(2,1)} %param.35) | copy-start | bytes 11010052
  185.1 5.2 %copy-start.2 = (bf16[256,128]{1,0:T(8,128)(2,1)S(1)}, bf16[256,128]{1,0:T(8,128)(2,1)}, u32[]{:S(2)}) copy-start(bf16[256,128]{1,0:T(8,128)(2,1)} %param.20) | copy-start | bytes 196612
  185.1 5.3 %copy-start.12 = (bf16[128]{0:T(256)(128)(2,1)S(1)}, bf16[128]{0:T(256)(128)(2,1)}, u32[]{:S(2)}) copy-start(bf16[128]{0:T(256)(128)(2,1)} %param.27) | copy-start | bytes 772
  185.1 5.5 %copy-start.3 = (bf16[256,64]{0,1:T(8,128)(2,1)S(1)}, bf16[256,64]{0,1:T(8,128)(2,1)}, u32[]{:S(2)}) copy-start(bf16[256,64]{0,1:T(8,128)(2,1)} %param.21) | copy-start | bytes 98308
  185.1 74.4 %all-to-all-start.3 = ((bf16[4,288,2048]{2,1,0:T(8,128)(2,1)}), bf16[4,288,2048]{2,1,0:T(8,128)(2,1)}, u32[]{:S(2)}, u32[]{:S(2)}) async-start(bf16[4,288,2048]{2,1,0:T(8,128)(2,1)} %bitcast.70), calls=%async_computation.3 | async-start | bytes 9437184 | tf_op jit(solution)/shard_map/all_to_all | solution.py:36
  259.5 18.3 %all-to-all-start = ((bf16[4,64,2048]{2,1,0:T(8,128)(2,1)}), bf16[4,64,2048]{2,1,0:T(8,128)(2,1)S(1)}, u32[]{:S(2)}, u32[]{:S(2)}) async-start(bf16[4,64,2048]{2,1,0:T(8,128)(2,1)} %bitcast.12), calls=%async_computation | async-start | bytes 2097152 | tf_op jit(solution)/shard_map/all_to_all | solution.py:36
  266.6 30.1 %copy-start.5 = (f32[128,2]{0,1:T(2,128)S(1)}, f32[128,2]{0,1:T(2,128)}, u32[]{:S(2)}) copy-start(f32[128,2]{0,1:T(2,128)} %param.32) | copy-start | bytes 3076
  277.9 117.5 %all-to-all-start.4 = ((bf16[32,9,2048]{2,1,0:T(8,128)(2,1)}), bf16[32,9,2048]{2,1,0:T(8,128)(2,1)}, u32[]{:S(2)}, u32[]{:S(2)}) async-start(bf16[32,9,2048]{2,1,0:T(8,128)(2,1)} %all_to_all.24), calls=%async_computation.4 | async-start | bytes 4194304 | tf_op jit(solution)/shard_map/all_to_all | solution.py:219
Sparse Core Ops, SparseCore 0:
  109.4 55.4 all-gather.4
  167.2 81.1 all-gather.2
where the time goes:
time: 414 us; the launch traced here: 413 us
  waiting for transfers between devices  219 us (53%)
  blocking collectives  85.9 us (21%)
  starting transfers between devices  27.9 us (7%)
  local copies, waits for them, and re-layouts  25.9 us (6%)
  matrix products  24.8 us (6%)
  other arithmetic  14.5 us (4%)
  between operations  14.5 us (4%)
    all_to_all x1, waiting for transfers between devices, experts(): lax.all_to_all(summed, EP, split_axis=0, concat_axis=0, tiled=True)  97.7 us
    all_to_all x2, blocking collectives, moved_by_axis(): lax.all_to_all(tiles, axes[k], split_axis=k, concat_axis=k, tiled=True)  85.9 us
    all_gather x1, waiting for transfers between devices, sent_together(): lax.all_gather(both, axis, axis=dim, tiled=True)  57.7 us
    all_gather x1, waiting for transfers between devices, experts(): piece = lax.all_gather(arrived, 'tp', axis=0, tiled=True)  53.7 us
    all_to_all x1, starting transfers between devices, experts(): lax.all_to_all(summed, EP, split_axis=0, concat_axis=0, tiled=True)  18.7 us
    all_to_all x2, waiting for transfers between devices, sum_at_owner(): tiles = lax.all_to_all(in_blocks(array, dim, size), axis, 0, 0, tiled=True)  9.7 us
    all_to_all x2, starting transfers between devices, sum_at_owner(): tiles = lax.all_to_all(in_blocks(array, dim, size), axis, 0, 0, tiled=True)  8.82 us
  transfers between devices with their start and end apart: 5, of which 4 were waited for; matrix products, arithmetic and copies ran while one was open for 9% of the time, Pallas kernels for 0%

commit v1 on v0

--- a/solution.py
+++ b/solution.py
@@ -205,7 +205,9 @@
     up_local = up_weight[0]
     down_local = down_weight[0]
     arrived = two_step_exchange(outgoing, ("ep_0", "ep_1"), (1, 0), 0, 0)
-    piece = lax.all_gather(arrived, "tp", axis=0, tiled=True)
+    piece = jnp.concatenate(
+        lax.all_to_all(jnp.stack([arrived] * lax.axis_size("tp")), "tp", 0, 0), axis=0
+    )
     gate = jnp.dot(piece, gate_local, preferred_element_type=jnp.float32)
     upward = jnp.dot(piece, up_local, preferred_element_type=jnp.float32)
     hidden = (jax.nn.silu(gate) * upward).astype(jnp.bfloat16)

time: 414 us -> 395 us (0.954)
  waiting for transfers between devices: 219 us -> 193 us
  starting transfers between devices: 27.9 us -> 42.9 us
  blocking collectives: 85.9 us -> 77.6 us
  local copies, waits for them, and re-layouts: 25.9 us -> 30.2 us
    all_to_all x2 -> x1, blocking collectives: 85.9 us -> 24.9 us  [moved_by_axis(): lax.all_to_all(tiles, axes[k], split_axis=k, concat_axis=k, tiled=True)]
    all_gather x1, waiting for transfers between devices: 57.7 us -> 0.02 us  [sent_together(): lax.all_gather(both, axis, axis=dim, tiled=True)]
    all_to_all x0 -> x1, waiting for transfers between devices: none -> 54.4 us  [moved_by_axis(): lax.all_to_all(tiles, axes[k], split_axis=k, concat_axis=k, tiled=True)]
    all_gather x1 -> x0, waiting for transfers between devices: 53.7 us -> none  [experts(): piece = lax.all_gather(arrived, 'tp', axis=0, tiled=True)]
    all_to_all x0 -> x1, blocking collectives: none -> 52.8 us  [experts(): lax.all_to_all(jnp.stack([arrived] * lax.axis_size('tp')), 'tp', 0, 0)]
    all_to_all x2, waiting for transfers between devices: 9.7 us -> 40.5 us  [sum_at_owner(): tiles = lax.all_to_all(in_blocks(array, dim, size), axis, 0, 0, tiled=True)]
    all_to_all x1, starting transfers between devices: 18.7 us -> 29.1 us  [experts(): lax.all_to_all(summed, EP, split_axis=0, concat_axis=0, tiled=True)]
    all_to_all x0 -> x1, starting transfers between devices: none -> 4.77 us  [moved_by_axis(): lax.all_to_all(tiles, axes[k], split_axis=k, concat_axis=k, tiled=True)]
  transfers between devices with their start and end apart: 5 -> 5, of which waited for: 4 -> 4; matrix products, arithmetic and copies ran while one was open for 9% -> 10% of each run, Pallas kernels for 0% -> 0%
where the time goes in v1:
time: 395 us; the launch traced here: 394 us
  waiting for transfers between devices  193 us (49%)
  blocking collectives  77.6 us (20%)
  starting transfers between devices  42.9 us (11%)
  local copies, waits for them, and re-layouts  30.2 us (8%)
  matrix products  21.8 us (6%)
  other arithmetic  14.5 us (4%)
  between operations  14.5 us (4%)
    all_to_all x1, waiting for transfers between devices, experts(): lax.all_to_all(summed, EP, split_axis=0, concat_axis=0, tiled=True)  97.7 us
    all_to_all x1, waiting for transfers between devices, moved_by_axis(): lax.all_to_all(tiles, axes[k], split_axis=k, concat_axis=k, tiled=True)  54.4 us
    all_to_all x1, blocking collectives, experts(): lax.all_to_all(jnp.stack([arrived] * lax.axis_size('tp')), 'tp', 0, 0)  52.8 us
    all_to_all x2, waiting for transfers between devices, sum_at_owner(): tiles = lax.all_to_all(in_blocks(array, dim, size), axis, 0, 0, tiled=True)  40.5 us
    all_to_all x1, starting transfers between devices, experts(): lax.all_to_all(summed, EP, split_axis=0, concat_axis=0, tiled=True)  29.1 us
    all_to_all x1, blocking collectives, moved_by_axis(): lax.all_to_all(tiles, axes[k], split_axis=k, concat_axis=k, tiled=True)  24.9 us
    all_to_all x2, starting transfers between devices, sum_at_owner(): tiles = lax.all_to_all(in_blocks(array, dim, size), axis, 0, 0, tiled=True)  8.98 us
  transfers between devices with their start and end apart: 5, of which 4 were waited for; matrix products, arithmetic and copies ran while one was open for 10% of the time, Pallas kernels for 0%

profile of v1, /device:TPU:33, one launch (start us, length us, event | category | flops | bytes accessed | tf_op | source)
XLA Modules:
  0.0 394.4 jit_solution(2050268525110073069)
XLA Ops:
  14.5 3.2 scatter_custom_fusion
  20.0 24.9 %all_to_all.37 = bf16[16,2,9,2048]{3,0,2,1:T(8,128)(2,1)S(1)} all-to-all(bf16[16,2,9,2048]{3,0,2,1:T(8,128)(2,1)S(1)} %copy.34), channel_id=1, replica_groups=mesh['grp'=2,'ep_0'=16,'ep_1'=2,'tp'=4] {'ep_1'}, dimensions={1} | all-to-all | bytes 2359296 | tf_op jit(solution)/shard_map/all_to_all | solution.py:50
  44.9 2.3 copy.35
  47.1 4.8 %all-to-all-start.2 = ((bf16[16,2,9,2048]{3,1,2,0:T(2,128)(2,1)}), bf16[16,2,9,2048]{3,1,2,0:T(2,128)(2,1)}, u32[]{:S(2)}, u32[]{:S(2)}) async-start(bf16[16,2,9,2048]{3,1,2,0:T(2,128)(2,1)} %copy.35), calls=%async_computation.2 | async-start | bytes 2359296 | tf_op jit(solution)/shard_map/all_to_all | solution.py:50
  53.7 54.4 %all-to-all-done.2 = bf16[16,2,9,2048]{3,1,2,0:T(2,128)(2,1)} async-done(((bf16[16,2,9,2048]{3,1,2,0:T(2,128)(2,1)}), bf16[16,2,9,2048]{3,1,2,0:T(2,128)(2,1)}, u32[]{:S(2)}, u32[]{:S(2)}) %all-to-all-start.2) | async-done | bytes 1179680 | tf_op jit(solution)/shard_map/all_to_all | solution.py:50
  108.1 1.9 copy.36
  111.4 1.9 stack.3
  113.3 52.8 %all_to_all.38 = bf16[4,288,2048]{2,1,0:T(8,128)(2,1)S(1)} all-to-all(bf16[4,288,2048]{2,1,0:T(8,128)(2,1)S(1)} %stack.3), channel_id=1, replica_groups=mesh['grp'=2,'ep_0'=16,'ep_1'=2,'tp'=4] {'tp'}, dimensions={0} | all-to-all | bytes 9437184 | tf_op jit(solution)/shard_map/all_to_all | solution.py:209
  166.1 5.1 %fusion.14 = f32[1152,896]{1,0:T(8,128)S(1)} fusion(bf16[1152,2048]{1,0:T(8,128)(2,1)S(1)} %bitcast.72, bf16[1,2048,896]{2,1,0:T(8,128)(2,1)S(1)} %copy-done.6), kind=kOutput, calls=%fused_computation.25 | convolution fusion | flops 4227858432 | bytes 12517376 | tf_op jit(solution)/shard_map/dot_general | solution.py:211
  171.2 5.3 %fusion.16 = bf16[1152,896]{1,0:T(8,128)(2,1)S(1)} fusion(bf16[1152,2048]{1,0:T(8,128)(2,1)S(1)} %bitcast.73, bf16[1,2048,896]{2,1,0:T(8,128)(2,1)S(1)} %copy-done.7, f32[1152,896]{1,0:T(8,128)S(1)} %fusion.14), kind=kOutput, calls=%fused_computation.27 | convolution fusion | flops 4234051584 | bytes 14581760 | tf_op jit(solution)/shard_map/dot_general | solution.py:212
  176.6 6.8 %convolution_convert_fusion = bf16[1152,2048]{1,0:T(8,128)(2,1)} fusion(bf16[1152,896]{1,0:T(8,128)(2,1)S(1)} %fusion.16, bf16[1,896,2048]{2,1,0:T(8,128)(2,1)S(1)} %copy-done.8), kind=kOutput, calls=%fused_computation.21 | convolution fusion | flops 4230217728 | bytes 10452992 | tf_op jit(solution)/shard_map/dot_general | solution.py:215
  183.3 5.2 %all-to-all-start.4 = ((bf16[4,288,2048]{2,1,0:T(8,128)(2,1)}), bf16[4,288,2048]{2,1,0:T(8,128)(2,1)}, u32[]{:S(2)}, u32[]{:S(2)}) async-start(bf16[4,288,2048]{2,1,0:T(8,128)(2,1)} %bitcast.71), calls=%async_computation.4 | async-start | bytes 9437184 | tf_op jit(solution)/shard_map/all_to_all | solution.py:36
  190.0 3.9 fusion.47
  193.9 4.5 %while.16 = (s32[]{:T(128)}, f32[256,2,64]{0,2,1:T(8,128)S(1)}, f32[256,2]{0,1:T(2,128)S(1)}, s32[]{:T(128)}, bf16[8192,128]{0,1:T(8,128)(2,1)}, /*index=5*/bf16...) while((s32[]{:T(128)}, f32[256,2,64]{0,2,1:T(8,128)S(1)}, ...), condition=%wide.region_5.6_spmd.clone, body=%wide.region_1.5_spmd.clone.sunk | while | flops 343476992 | bytes 22022456 | solution.py:158
  194.0 4.3 %conditional.3 = ((f32[256,2,64]{0,2,1:T(8,128)S(1)}, f32[256,2]{0,1:T(2,128)S(1)})) conditional(s32[]{:T(128)} %convert_element_type.210, (s32[]{:T(128)}, s32[]{:T(128)}, bf16[8192,128]{0,1:T(8,128)(2,1)}, bf16[256,2,64]{0,2,1:T(8,128)(2,1)S(1)}, bf16[8192,32]{0,1:T(8,128)(2,1)S(1)}, /*index=5*/bf16[256,2,32]{0,2,1:T(8,128)(2,1)S(1)}, ...), branch_computations={%region_2.3_spmd, %region_4.4_spmd} | conditional | flops 343476992 | bytes 22021194 | solution.py:146
  200.0 36.0 %all-to-all-done.4 = bf16[4,288,2048]{2,1,0:T(8,128)(2,1)} async-done(((bf16[4,288,2048]{2,1,0:T(8,128)(2,1)}), bf16[4,288,2048]{2,1,0:T(8,128)(2,1)}, u32[]{:S(2)}, u32[]{:S(2)}) %all-to-all-start.4) | async-done | bytes 4718624 | tf_op jit(solution)/shard_map/all_to_all | solution.py:36
  236.1 3.8 all-to-all-start
  239.9 3.3 reduce_sum.74
  244.8 4.5 %all-to-all-done = bf16[4,64,2048]{2,1,0:T(8,128)(2,1)S(1)} async-done(((bf16[4,64,2048]{2,1,0:T(8,128)(2,1)}), bf16[4,64,2048]{2,1,0:T(8,128)(2,1)S(1)}, u32[]{:S(2)}, u32[]{:S(2)}) %all-to-all-start) | async-done | bytes 1048608 | tf_op jit(solution)/shard_map/all_to_all | solution.py:36
  249.3 29.1 %all-to-all-start.5 = ((bf16[32,9,2048]{2,1,0:T(8,128)(2,1)}), bf16[32,9,2048]{2,1,0:T(8,128)(2,1)}, u32[]{:S(2)}, u32[]{:S(2)}) async-start(bf16[32,9,2048]{2,1,0:T(8,128)(2,1)} %all_to_all.28), calls=%async_computation.5 | async-start | bytes 4194304 | tf_op jit(solution)/shard_map/all_to_all | solution.py:221
  279.4 97.7 %all-to-all-done.5 = bf16[32,9,2048]{2,1,0:T(8,128)(2,1)} async-done(((bf16[32,9,2048]{2,1,0:T(8,128)(2,1)}), bf16[32,9,2048]{2,1,0:T(8,128)(2,1)}, u32[]{:S(2)}, u32[]{:S(2)}) %all-to-all-start.5) | async-done | bytes 1179680 | tf_op jit(solution)/shard_map/all_to_all | solution.py:221
  378.9 2.3 gather_fusion
  381.3 2.4 reshape.303
  383.6 3.9 multiply_reduce_fusion
  (93 shorter events, 24.3 us)
Async XLA Ops:
  7.2 191.4 %copy-start = (bf16[128,2048]{1,0:T(8,128)(2,1)S(1)}, bf16[128,2048]{1,0:T(8,128)(2,1)}, u32[]{:S(2)}) copy-start(bf16[128,2048]{1,0:T(8,128)(2,1)} %param.28) | copy-start | bytes 1572868
  20.0 32.0 %copy-start.11 = (bf16[256]{0:T(256)(128)(2,1)S(1)}, bf16[256]{0:T(256)(128)(2,1)}, u32[]{:S(2)}) copy-start(bf16[256]{0:T(256)(128)(2,1)} %param.26) | copy-start | bytes 1540
  20.0 32.1 %copy-start.1 = (bf16[256,256]{1,0:T(8,128)(2,1)S(1)}, bf16[256,256]{1,0:T(8,128)(2,1)}, u32[]{:S(2)}) copy-start(bf16[256,256]{1,0:T(8,128)(2,1)} %param.22) | copy-start | bytes 393220
  20.0 32.2 %copy-start.4 = (bf16[256,32]{0,1:T(8,128)(2,1)S(1)}, bf16[256,32]{0,1:T(8,128)(2,1)}, u32[]{:S(2)}) copy-start(bf16[256,32]{0,1:T(8,128)(2,1)} %param.23) | copy-start | bytes 49156
  20.0 32.4 %copy-start.9 = (bf16[256,128]{1,0:T(8,128)(2,1)S(1)}, bf16[256,128]{1,0:T(8,128)(2,1)}, u32[]{:S(2)}) copy-start(bf16[256,128]{1,0:T(8,128)(2,1)} %param.25) | copy-start | bytes 196612
  20.0 32.6 %copy-start.10 = (bf16[256,128]{1,0:T(8,128)(2,1)S(1)}, bf16[256,128]{1,0:T(8,128)(2,1)}, u32[]{:S(2)}) copy-start(bf16[256,128]{1,0:T(8,128)(2,1)} %param.24) | copy-start | bytes 196612
  47.1 60.9 %all-to-all-start.2 = ((bf16[16,2,9,2048]{3,1,2,0:T(2,128)(2,1)}), bf16[16,2,9,2048]{3,1,2,0:T(2,128)(2,1)}, u32[]{:S(2)}, u32[]{:S(2)}) async-start(bf16[16,2,9,2048]{3,1,2,0:T(2,128)(2,1)} %copy.35), calls=%async_computation.2 | async-start | bytes 2359296 | tf_op jit(solution)/shard_map/all_to_all | solution.py:50
  51.9 137.0 %all-gather.2.cloned.1.call-start = ((), (), s32[]{:S(2)}) async-start(), calls=%async_computation.6 | async-start | bytes 4866048 | tf_op jit(solution)/shard_map/all_gather | solution.py:25
  113.3 52.8 %copy-start.6 = (bf16[1,2048,896]{2,1,0:T(8,128)(2,1)S(1)}, bf16[1,2048,896]{2,1,0:T(8,128)(2,1)}, u32[]{:S(2)}) copy-start(bf16[1,2048,896]{2,1,0:T(8,128)(2,1)} %param.33) | copy-start | bytes 11010052
  166.1 5.1 %copy-start.7 = (bf16[1,2048,896]{2,1,0:T(8,128)(2,1)S(1)}, bf16[1,2048,896]{2,1,0:T(8,128)(2,1)}, u32[]{:S(2)}) copy-start(bf16[1,2048,896]{2,1,0:T(8,128)(2,1)} %param.34) | copy-start | bytes 11010052
  171.2 5.3 %copy-start.8 = (bf16[1,896,2048]{2,1,0:T(8,128)(2,1)S(1)}, bf16[1,896,2048]{2,1,0:T(8,128)(2,1)}, u32[]{:S(2)}) copy-start(bf16[1,896,2048]{2,1,0:T(8,128)(2,1)} %param.35) | copy-start | bytes 11010052
  183.3 5.2 %copy-start.2 = (bf16[256,128]{1,0:T(8,128)(2,1)S(1)}, bf16[256,128]{1,0:T(8,128)(2,1)}, u32[]{:S(2)}) copy-start(bf16[256,128]{1,0:T(8,128)(2,1)} %param.20) | copy-start | bytes 196612
  183.3 5.3 %copy-start.12 = (bf16[128]{0:T(256)(128)(2,1)S(1)}, bf16[128]{0:T(256)(128)(2,1)}, u32[]{:S(2)}) copy-start(bf16[128]{0:T(256)(128)(2,1)} %param.27) | copy-start | bytes 772
  183.3 5.5 %copy-start.3 = (bf16[256,64]{0,1:T(8,128)(2,1)S(1)}, bf16[256,64]{0,1:T(8,128)(2,1)}, u32[]{:S(2)}) copy-start(bf16[256,64]{0,1:T(8,128)(2,1)} %param.21) | copy-start | bytes 98308
  183.3 52.7 %all-to-all-start.4 = ((bf16[4,288,2048]{2,1,0:T(8,128)(2,1)}), bf16[4,288,2048]{2,1,0:T(8,128)(2,1)}, u32[]{:S(2)}, u32[]{:S(2)}) async-start(bf16[4,288,2048]{2,1,0:T(8,128)(2,1)} %bitcast.71), calls=%async_computation.4 | async-start | bytes 9437184 | tf_op jit(solution)/shard_map/all_to_all | solution.py:36
  236.1 13.3 %all-to-all-start = ((bf16[4,64,2048]{2,1,0:T(8,128)(2,1)}), bf16[4,64,2048]{2,1,0:T(8,128)(2,1)S(1)}, u32[]{:S(2)}, u32[]{:S(2)}) async-start(bf16[4,64,2048]{2,1,0:T(8,128)(2,1)} %bitcast.12), calls=%async_computation | async-start | bytes 2097152 | tf_op jit(solution)/shard_map/all_to_all | solution.py:36
  243.2 35.2 %copy-start.5 = (f32[128,2]{0,1:T(2,128)S(1)}, f32[128,2]{0,1:T(2,128)}, u32[]{:S(2)}) copy-start(f32[128,2]{0,1:T(2,128)} %param.32) | copy-start | bytes 3076
  249.3 127.8 %all-to-all-start.5 = ((bf16[32,9,2048]{2,1,0:T(8,128)(2,1)}), bf16[32,9,2048]{2,1,0:T(8,128)(2,1)}, u32[]{:S(2)}, u32[]{:S(2)}) async-start(bf16[32,9,2048]{2,1,0:T(8,128)(2,1)} %all_to_all.28), calls=%async_computation.5 | async-start | bytes 4194304 | tf_op jit(solution)/shard_map/all_to_all | solution.py:221
Sparse Core Ops, SparseCore 0:
  55.1 107.9 all-gather.1
